TPU v7x, 32 devices: a whole 2x2x4 slice. The times are simulated.
32 devices in a mesh: fs: 4 (over y, x), tp: 8 (over z, core).
Axes of the slice: x: 2, y: 2, z: 4, core: 2. Of those that a mesh axis runs over, the one named last changes fastest.
Arguments:
- hidden_in: bfloat16 [6144, 4096], P('fs', 'tp'), may hold values from -6 to 6
- forget_pre: bfloat16 [6144, 2048], P('fs', 'tp'), may hold values from -8 to 8
- forget_cot: bfloat16 [6144, 2048], P('fs', 'tp'), may hold values from -0.4375 to 0.4375
- lower_bound: float32 [2048], P('tp'), may hold values from 0.05 to 0.9
- head_out: bfloat16 [6144, 2048], P('fs', 'tp'), may hold values from -6 to 6
- out_cot: bfloat16 [6144, 4096], P('fs', 'tp'), may hold values from -0.109375 to 0.109375
- basis_forget: bfloat16 [2048, 256], replicated, may hold values from -0.37565048 to 0.37565048
- basis_output: bfloat16 [2048, 256], replicated, may hold values from -0.37565048 to 0.37565048
- weight_forget: float32 [2048, 4096], P('fs', 'tp'), may hold values from -0.09375 to 0.09375
- weight_output: float32 [4096, 2048], P('tp', 'fs'), may hold values from -0.125 to 0.125
- mean_forget: float32 [256, 4096], P('fs', 'tp'), may hold values from -3.5 to 3.5
- var_forget: float32 [256, 4096], P('fs', 'tp'), may hold values from 0.003 to 0.05
- mean_output: float32 [256, 4096], P('fs', 'tp'), may hold values from -3.5 to 3.5
- var_output: float32 [256, 4096], P('fs', 'tp'), may hold values from 0.003 to 0.05
Outputs:
- step_forget: float32 [2048, 4096], P('fs', 'tp')
- step_output: float32 [4096, 2048], P('tp', 'fs')
- new_forget: float32 [2048, 4096], P('fs', 'tp')
- new_output: float32 [4096, 2048], P('tp', 'fs')
- mean_forget_new: float32 [256, 4096], P('fs', 'tp')
- var_forget_new: float32 [256, 4096], P('fs', 'tp')
- mean_output_new: float32 [256, 4096], P('fs', 'tp')
- var_output_new: float32 [256, 4096], P('fs', 'tp')
- copy_forget: bfloat16 [2048, 4096], P(None, 'tp')
- copy_output: bfloat16 [4096, 2048], P('tp')
All inputs are finite; a program needn't handle non-finite values.
Results may differ from a plain program's by a relative error of at most 0.014.
Values may be sent and summed in bfloat16 or wider, within the bound.
A program may use at most 64 MiB of HBM per device.

v0:
```python
import jax
import jax.numpy as jnp
from jax import lax
from jax.sharding import PartitionSpec as P

D = 4096
HW = 2048
beta_one = 0.9
beta_two = 0.99
adam_eps = 1e-08
norm_eps = 1e-06
step_rate = 0.02


def moment_update(mean, var, proj):
    mean_new = beta_one * mean + (1.0 - beta_one) * proj
    var_new = beta_two * var + (1.0 - beta_two) * proj * proj
    return (mean_new, var_new, mean_new / (jnp.sqrt(var_new) + adam_eps))


def split_product(coords, tokens_data):
    upper = coords.astype(jnp.bfloat16)
    lower = (coords - upper.astype(jnp.float32)).astype(jnp.bfloat16)
    first = jnp.einsum("tr,td->rd", upper, tokens_data, preferred_element_type=jnp.float32)
    second = jnp.einsum("tr,td->rd", lower, tokens_data, preferred_element_type=jnp.float32)
    return first + second


def per_device(
    hidden_in,
    forget_pre,
    forget_cot,
    lower_bound,
    head_out,
    out_cot,
    basis_forget,
    basis_output,
    weight_forget,
    weight_output,
    mean_forget,
    var_forget,
    mean_output,
    var_output,
):
    highest = lax.Precision.HIGHEST
    fs_rank = lax.axis_index("fs")
    tp_rank = lax.axis_index("tp")
    unit_count = forget_pre.shape[1]
    feat_cols = hidden_in.shape[1]
    head_rows = weight_forget.shape[0]
    sigmoid_z = jax.nn.sigmoid(forget_pre.astype(jnp.float32))
    keep_rate = 1.0 - lower_bound
    forget_val = lower_bound + keep_rate * sigmoid_z
    gate_grad = (
        forget_cot.astype(jnp.float32) * keep_rate * sigmoid_z * (1.0 - sigmoid_z) / forget_val
    ).astype(jnp.bfloat16)
    rows_forget = lax.dynamic_slice_in_dim(basis_forget, fs_rank * head_rows, head_rows, 0).astype(
        jnp.float32
    )
    rows_output = lax.dynamic_slice_in_dim(basis_output, fs_rank * head_rows, head_rows, 0).astype(
        jnp.float32
    )
    local_forget = lax.dynamic_slice_in_dim(basis_forget, tp_rank * unit_count, unit_count, 0)
    local_output = lax.dynamic_slice_in_dim(basis_output, tp_rank * unit_count, unit_count, 0)
    coords_forget = jnp.dot(gate_grad, local_forget, preferred_element_type=jnp.float32)
    coords_output = jnp.dot(head_out, local_output, preferred_element_type=jnp.float32)
    coords_forget, coords_output = lax.psum((coords_forget, coords_output), "tp")
    part_forget = split_product(coords_forget, hidden_in)
    part_output = split_product(coords_output, out_cot)
    proj = lax.psum_scatter(
        jnp.concatenate([part_forget, part_output], axis=1), "fs", scatter_dimension=0, tiled=True
    )
    mean_f, var_f, dir_forget = moment_update(mean_forget, var_forget, proj[:, :feat_cols])
    mean_o, var_o, dir_output = moment_update(mean_output, var_output, proj[:, feat_cols:])
    dir_forget, dir_output = (
        lax.all_gather(dir_forget, "fs", axis=0, tiled=True),
        lax.all_gather(dir_output, "fs", axis=0, tiled=True),
    )
    upd_forget = jnp.dot(rows_forget, dir_forget, precision=highest)
    upd_output = jnp.dot(rows_output, dir_output, precision=highest)
    total = float(HW * D)
    sum_forget, sum_output = lax.psum(
        (jnp.sum(upd_forget * upd_forget), jnp.sum(upd_output * upd_output)), ("fs", "tp")
    )
    step_forget = upd_forget * lax.rsqrt(sum_forget / total + norm_eps)
    step_output = (upd_output * lax.rsqrt(sum_output / total + norm_eps)).T
    new_forget = weight_forget - step_rate * step_forget
    new_output = weight_output - step_rate * step_output
    copy_forget, copy_output = (
        lax.all_gather(new_forget.astype(jnp.bfloat16), "fs", axis=0, tiled=True),
        lax.all_gather(new_output.astype(jnp.bfloat16), "fs", axis=1, tiled=True),
    )
    return (
        step_forget,
        step_output,
        new_forget,
        new_output,
        mean_f,
        var_f,
        mean_o,
        var_o,
        copy_forget,
        copy_output,
    )


def solution(mesh):
    return jax.shard_map(
        per_device,
        mesh=mesh,
        in_specs=(
            P("fs", "tp"),
            P("fs", "tp"),
            P("fs", "tp"),
            P("tp"),
            P("fs", "tp"),
            P("fs", "tp"),
            P(),
            P(),
            P("fs", "tp"),
            P("tp", "fs"),
            P("fs", "tp"),
            P("fs", "tp"),
            P("fs", "tp"),
            P("fs", "tp"),
        ),
        out_specs=(
            P("fs", "tp"),
            P("tp", "fs"),
            P("fs", "tp"),
            P("tp", "fs"),
            P("fs", "tp"),
            P("fs", "tp"),
            P("fs", "tp"),
            P("fs", "tp"),
            P(None, "tp"),
            P("tp", None),
        ),
        check_vma=False,
    )
```

profile of v0, /device:TPU:0, one launch (start us, length us, event | category | flops | bytes accessed | tf_op | source)
XLA Modules:
  0.0 282.4 jit_solution(18277025858053126377)
XLA Ops:
  7.2 0.0 copy-start
  7.2 0.0 copy-start.9
  7.2 0.0 copy-start.11
  7.2 0.0 copy-start.10
  7.2 0.0 all-reduce.4.cloned.1.call-start
  7.3 0.8 broadcast_subtract_fusion
  8.1 2.8 convolution_bitcast_fusion
  10.9 0.0 copy-done.9
  10.9 0.0 copy-done.11
  10.9 0.0 copy-done.10
  10.9 3.0 %fusion = f32[1536,256]{1,0:T(8,128)} fusion(bf16[1536,256]{1,0:T(8,128)(2,1)S(1)} %copy-done.10, bf16[1536,256]{1,0:T(8,128)(2,1)S(1)} %copy-done.11, f32[256]{0:T(256)S(1)} %copy-done.9, f32[256]{0:T(256)S(1)} %broadcast_subtract_fusion, bf16[2048,256]{1,0:T(8,128)(2,1)} %param.20, s32[]{:T(128)S(6)} %select_n.9), kind=kOutput, calls=%fused_computation.12 | convolution fusion | flops 206438400 | bytes 3278852 | tf_op jit(solution)/shard_map/dot_general | solution.py:65
  13.9 0.0 all-reduce.4.cloned.1.call-update
  13.9 0.0 reduce-scatter.2.cloned.1.call-start
  13.9 79.7 %all-reduce.4.cloned.1.call-done = (f32[1536,256]{0,1:T(8,128)}, f32[1536,256]{1,0:T(8,128)}) async-done(((f32[1536,256]{0,1:T(8,128)}, f32[1536,256]{1,0:T(8,128)}), (f32[1536,256]{0,1:T(8,128)}, f32[1536,256]{1,0:T(8,128)})) %all-reduce.4.cloned.1.call-update) | async-done | bytes 3145744 | tf_op jit(solution)/shard_map/psum | solution.py:67
  93.7 2.1 fusion.2
  95.8 0.0 copy-done.3
  95.8 0.0 copy-start.1
  95.8 0.6 convolution_add_fusion
  96.4 0.8 copy-done.1
  97.2 0.5 copy-done.2
  97.7 0.6 fusion.5
  98.3 0.6 convolution_add_fusion.1
  98.9 0.0 copy-start.5
  98.9 0.0 copy-start.6
  98.9 0.0 copy-start.7
  98.9 0.0 copy-start.8
  98.9 1.1 pad_maximum_fusion
  100.0 0.0 reduce-scatter.2.cloned.1.call-update
  100.0 0.0 all-gather.3.cloned.1.call-start
  100.1 28.0 %reduce-scatter.2.cloned.1.call-done = f32[64,1024]{1,0:T(8,128)} async-done(((f32[256,1024]{1,0:T(8,128)}), f32[64,1024]{1,0:T(8,128)}) %reduce-scatter.2.cloned.1.call-update) | async-done | bytes 262160 | tf_op jit(solution)/shard_map/reduce_scatter | solution.py:70
  128.0 0.0 copy-done.5
  128.0 1.9 add_divide_fusion
  129.9 10.1 %all_gather.13 = f32[256,512]{1,0:T(8,128)S(1)} all-gather(f32[64,512]{1,0:T(8,128)S(1)} %get-tuple-element.20), channel_id=1, replica_groups=mesh['fs'=4,'tp'=8] {'fs'}, dimensions={0}, use_global_device_ids=true | all-gather | bytes 655360 | tf_op jit(solution)/shard_map/all_gather | solution.py:77
  140.0 9.7 %all_gather.12 = f32[256,512]{1,0:T(8,128)S(1)} all-gather(f32[64,512]{1,0:T(8,128)S(1)} %get-tuple-element.26), channel_id=1, replica_groups=mesh['fs'=4,'tp'=8] {'fs'}, dimensions={0}, use_global_device_ids=true | all-gather | bytes 655360 | tf_op jit(solution)/shard_map/all_gather | solution.py:76
  149.7 2.3 multiply_reduce_fusion.1
  152.0 3.2 %multiply_reduce_fusion = (f32[]{:T(128)}, f32[512,512]{1,0:T(8,128)}) fusion(f32[256,512]{1,0:T(8,128)S(1)} %all_gather.13, bf16[2048,256]{1,0:T(8,128)(2,1)} %param.21, s32[]{:T(128)S(6)} %select_n.8), kind=kOutput, calls=%fused_computation.10 | convolution fusion | flops 805830656 | bytes 1835016 | tf_op jit(solution)/shard_map/dot_general | solution.py:80
  155.1 39.5 %all-reduce = (f32[]{:T(128)}, f32[]{:T(128)}) all-reduce(f32[]{:T(128)} %get-tuple-element.29, f32[]{:T(128)} %get-tuple-element.31), channel_id=1, replica_groups=mesh['fs'=4,'tp'=8] {'fs','tp'}, use_global_device_ids=true, to_apply=%region_4.0 | all-reduce | flops 2 | bytes 16 | tf_op jit(solution)/shard_map/psum | solution.py:82
  195.4 3.1 %fusion.21 = (bf16[512,512]{1,0:T(8,128)(2,1)}, f32[512,512]{1,0:T(8,128)}, f32[512,512]{1,0:T(8,128)}) fusion(f32[512,512]{1,0:T(8,128)} %param.22, f32[512,512]{1,0:T(8,128)S(1)} %get-tuple-element.30, f32[]{:T(128)S(6)} %rsqrt.6), kind=kLoop, calls=%fused_computation.41 | loop fusion | flops 1048576 | bytes 4718596 | tf_op jit(solution)/shard_map/convert_element_type | solution.py:90
  198.4 0.0 all-gather.3.cloned.1.call-update
  198.5 0.0 all-gather.5.cloned.1.call-start
  198.5 1.6 copy.24
  200.8 3.1 %fusion.20 = (bf16[512,512]{1,0:T(8,128)(2,1)}, f32[512,512]{1,0:T(8,128)}, f32[512,512]{1,0:T(8,128)}) fusion(f32[512,512]{1,0:T(8,128)} %param.23, f32[512,512]{0,1:T(8,128)S(1)} %copy.24, f32[]{:T(128)S(6)} %rsqrt.7), kind=kLoop, calls=%fused_computation.40 | loop fusion | flops 1048576 | bytes 4718596 | tf_op jit(solution)/shard_map/convert_element_type | solution.py:91
  203.9 0.0 all-gather.5.cloned.1.call-update
  203.9 30.1 %all-gather.3.cloned.1.call-done = bf16[2048,512]{1,0:T(8,128)(2,1)} async-done(((bf16[512,512]{1,0:T(8,128)(2,1)}), bf16[2048,512]{1,0:T(8,128)(2,1)}) %all-gather.3.cloned.1.call-update) | async-done | bytes 2097168 | tf_op jit(solution)/shard_map/all_gather | solution.py:90
  234.0 37.3 %all-gather.5.cloned.1.call-done = bf16[512,2048]{1,0:T(8,128)(2,1)} async-done(((bf16[512,512]{1,0:T(8,128)(2,1)}), bf16[512,2048]{1,0:T(8,128)(2,1)}) %all-gather.5.cloned.1.call-update) | async-done | bytes 2097168 | tf_op jit(solution)/shard_map/all_gather | solution.py:91
  271.4 3.2 %copy.29 = bf16[2048,512]{1,0:T(8,128)(2,1)} copy(bf16[2048,512]{1,0:T(8,128)(2,1)} %all-gather.3.cloned.1.call-done) | data formatting | bytes 4194304
  274.6 0.0 copy-done.4
  274.6 1.3 copy.30
  (7 shorter events, 0.0 us)
Async XLA Ops:
  7.2 86.5 %copy-start = (bf16[1536,512]{1,0:T(8,128)(2,1)S(1)}, bf16[1536,512]{1,0:T(8,128)(2,1)}, u32[]{:S(2)}) copy-start(bf16[1536,512]{1,0:T(8,128)(2,1)} %param.19) | copy-start | bytes 4718596
  7.2 3.7 %copy-start.9 = (f32[256]{0:T(256)S(1)}, f32[256]{0:T(256)}, u32[]{:S(2)}) copy-start(f32[256]{0:T(256)} %param.17) | copy-start | bytes 3076
  7.2 3.7 %copy-start.11 = (bf16[1536,256]{1,0:T(8,128)(2,1)S(1)}, bf16[1536,256]{1,0:T(8,128)(2,1)}, u32[]{:S(2)}) copy-start(bf16[1536,256]{1,0:T(8,128)(2,1)} %param.16) | copy-start | bytes 2359300
  7.2 3.7 %copy-start.10 = (bf16[1536,256]{1,0:T(8,128)(2,1)S(1)}, bf16[1536,256]{1,0:T(8,128)(2,1)}, u32[]{:S(2)}) copy-start(bf16[1536,256]{1,0:T(8,128)(2,1)} %param.15) | copy-start | bytes 2359300
  7.2 86.4 %all-reduce.4.cloned.1.call-start = ((), (), s32[]{:S(2)}) async-start(), calls=%async_computation.4 | async-start | bytes 6291456 | tf_op jit(solution)/shard_map/psum | solution.py:67
  13.9 114.1 %reduce-scatter.2.cloned.1.call-start = ((), (), s32[]{:S(2)}) async-start(), calls=%async_computation.1 | async-start | bytes 1310720 | tf_op jit(solution)/shard_map/reduce_scatter | solution.py:70
  93.7 2.1 copy-start.3
  95.8 1.4 copy-start.1
  95.8 1.9 copy-start.2
  98.9 29.2 %copy-start.5 = (f32[64,512]{1,0:T(8,128)S(1)}, f32[64,512]{1,0:T(8,128)}, u32[]{:S(2)}) copy-start(f32[64,512]{1,0:T(8,128)} %param.27) | copy-start | bytes 393220
  98.9 29.2 %copy-start.6 = (f32[64,512]{1,0:T(8,128)S(1)}, f32[64,512]{1,0:T(8,128)}, u32[]{:S(2)}) copy-start(f32[64,512]{1,0:T(8,128)} %param.26) | copy-start | bytes 393220
  98.9 29.1 %copy-start.7 = (f32[64,512]{1,0:T(8,128)S(1)}, f32[64,512]{1,0:T(8,128)}, u32[]{:S(2)}) copy-start(f32[64,512]{1,0:T(8,128)} %param.25) | copy-start | bytes 393220
  98.9 29.1 %copy-start.8 = (f32[64,512]{1,0:T(8,128)S(1)}, f32[64,512]{1,0:T(8,128)}, u32[]{:S(2)}) copy-start(f32[64,512]{1,0:T(8,128)} %param.24) | copy-start | bytes 393220
  100.0 134.0 %all-gather.3.cloned.1.call-start = ((), (), s32[]{:S(2)}) async-start(), calls=%async_computation.2 | async-start | bytes 2621440 | tf_op jit(solution)/shard_map/all_gather | solution.py:90
  198.5 72.9 %all-gather.5.cloned.1.call-start = ((), (), s32[]{:S(2)}) async-start(), calls=%async_computation.3 | async-start | bytes 2621440 | tf_op jit(solution)/shard_map/all_gather | solution.py:91
  271.4 3.2 %copy-start.4 = (bf16[512,2048]{1,0:T(8,128)(2,1)S(1)}, bf16[512,2048]{1,0:T(8,128)(2,1)}, u32[]{:S(2)}) copy-start(bf16[512,2048]{1,0:T(8,128)(2,1)} %all-gather.5.cloned.1.call-done) | copy-start | bytes 6291460
Sparse Core Ops, SparseCore 0:
  14.0 79.5 all-reduce.3
  100.1 27.8 reduce-scatter.1
  198.6 35.3 all-gather.2
  236.3 35.0 all-gather.4
where the time goes:
time: 283 us; the launch traced here: 282 us
  waiting for transfers between devices  175 us (62%)
  blocking collectives  59.3 us (21%)
  between operations  15.3 us (5%)
  matrix products  15.1 us (5%)
  other arithmetic  9.91 us (4%)
  local copies, waits for them, and re-layouts  7.41 us (3%)
    psum x1, waiting for transfers between devices, per_device(): lax.psum((coords_forget, coords_output), 'tp')  79.7 us
    psum x1, blocking collectives, per_device(): lax.psum((jnp.sum(upd_forget * upd_forget), jnp.sum(upd_output * upd_outp...  39.5 us
    all_gather x1, waiting for transfers between devices, per_device(): lax.all_gather(new_output.astype(jnp.bfloat16), 'fs', axis=1, tiled=True)  37.3 us
    all_gather x1, waiting for transfers between devices, per_device(): lax.all_gather(new_forget.astype(jnp.bfloat16), 'fs', axis=0, tiled=True)  30.1 us
    reduce_scatter x1, waiting for transfers between devices, per_device(): lax.psum_scatter(jnp.concatenate([part_forget, part_output], axis=1), 'fs...  28 us
    all_gather x1, blocking collectives, per_device(): lax.all_gather(dir_output, 'fs', axis=0, tiled=True)  10.1 us
    all_gather x1, blocking collectives, per_device(): lax.all_gather(dir_forget, 'fs', axis=0, tiled=True)  9.67 us
    unnamed x26, local copies, waits for them, and re-layouts  5.86 us
  transfers between devices with their start and end apart: 4, of which 4 were waited for; matrix products, arithmetic and copies ran while one was open for 2% of the time, Pallas kernels for 0%

commit v1 on v0

--- a/solution.py
+++ b/solution.py
@@ -10,6 +10,10 @@
 adam_eps = 1e-08
 norm_eps = 1e-06
 step_rate = 0.02
+
+
+def _create_leaves(frame_in):
+    return lax.psum(lax.psum(frame_in, "tp"), "fs")
 
 
 def moment_update(mean, var, proj):
@@ -79,8 +83,8 @@
     upd_forget = jnp.dot(rows_forget, dir_forget, precision=highest)
     upd_output = jnp.dot(rows_output, dir_output, precision=highest)
     total = float(HW * D)
-    sum_forget, sum_output = lax.psum(
-        (jnp.sum(upd_forget * upd_forget), jnp.sum(upd_output * upd_output)), ("fs", "tp")
+    sum_forget, sum_output = _create_leaves(
+        (jnp.sum(upd_forget * upd_forget), jnp.sum(upd_output * upd_output))
     )
     step_forget = upd_forget * lax.rsqrt(sum_forget / total + norm_eps)
     step_output = (upd_output * lax.rsqrt(sum_output / total + norm_eps)).T

time: 283 us -> 264 us (0.933)
  blocking collectives: 59.3 us -> 43.5 us
  waiting for transfers between devices: 175 us -> 172 us
    psum x1 -> x2, blocking collectives: 39.5 us -> 23.8 us  [_create_leaves(): return lax.psum(lax.psum(frame_in, 'tp'), 'fs')]
    all_gather x1, waiting for transfers between devices: 30.1 us -> 26.5 us  [per_device(): lax.all_gather(new_forget.astype(jnp.bfloat16), 'fs', axis=0, tiled=True)]
where the time goes in v1:
time: 264 us; the launch traced here: 263 us
  waiting for transfers between devices  172 us (65%)
  blocking collectives  43.5 us (16%)
  between operations  15.3 us (6%)
  matrix products  15.1 us (6%)
  other arithmetic  9.97 us (4%)
  local copies, waits for them, and re-layouts  7.41 us (3%)
    psum x1, waiting for transfers between devices, per_device(): lax.psum((coords_forget, coords_output), 'tp')  79.7 us
    all_gather x1, waiting for transfers between devices, per_device(): lax.all_gather(new_output.astype(jnp.bfloat16), 'fs', axis=1, tiled=True)  37.3 us
    reduce_scatter x1, waiting for transfers between devices, per_device(): lax.psum_scatter(jnp.concatenate([part_forget, part_output], axis=1), 'fs...  28 us
    all_gather x1, waiting for transfers between devices, per_device(): lax.all_gather(new_forget.astype(jnp.bfloat16), 'fs', axis=0, tiled=True)  26.5 us
    psum x2, blocking collectives, _create_leaves(): return lax.psum(lax.psum(frame_in, 'tp'), 'fs')  23.8 us
    all_gather x1, blocking collectives, per_device(): lax.all_gather(dir_output, 'fs', axis=0, tiled=True)  10.1 us
    all_gather x1, blocking collectives, per_device(): lax.all_gather(dir_forget, 'fs', axis=0, tiled=True)  9.67 us
    unnamed x26, local copies, waits for them, and re-layouts  5.86 us
  transfers between devices with their start and end apart: 4, of which 4 were waited for; matrix products, arithmetic and copies ran while one was open for 2% of the time, Pallas kernels for 0%

profile of v1, /device:TPU:0, one launch (start us, length us, event | category | flops | bytes accessed | tf_op | source)
XLA Modules:
  0.0 263.1 jit_solution(5047284948646170643)
XLA Ops:
  7.2 0.0 copy-start
  7.2 0.0 copy-start.9
  7.2 0.0 copy-start.11
  7.2 0.0 copy-start.10
  7.2 0.0 all-reduce.5.cloned.1.call-start
  7.3 0.8 broadcast_subtract_fusion
  8.1 2.8 %convolution_bitcast_fusion = f32[1536,256]{0,1:T(8,128)} fusion(bf16[1536,256]{1,0:T(8,128)(2,1)} %param.18, bf16[2048,256]{1,0:T(8,128)(2,1)} %param.21, s32[]{:T(128)S(6)} %select_n.9), kind=kOutput, calls=%fused_computation | convolution fusion | flops 201326592 | bytes 2490372 | tf_op jit(solution)/shard_map/dot_general | solution.py:70
  10.9 0.0 copy-done.9
  10.9 0.0 copy-done.11
  10.9 0.0 copy-done.10
  10.9 3.0 %fusion = f32[1536,256]{1,0:T(8,128)} fusion(bf16[1536,256]{1,0:T(8,128)(2,1)S(1)} %copy-done.10, bf16[1536,256]{1,0:T(8,128)(2,1)S(1)} %copy-done.11, f32[256]{0:T(256)S(1)} %copy-done.9, f32[256]{0:T(256)S(1)} %broadcast_subtract_fusion, bf16[2048,256]{1,0:T(8,128)(2,1)} %param.20, s32[]{:T(128)S(6)} %select_n.9), kind=kOutput, calls=%fused_computation.12 | convolution fusion | flops 206438400 | bytes 3278852 | tf_op jit(solution)/shard_map/dot_general | solution.py:69
  13.9 0.0 all-reduce.5.cloned.1.call-update
  13.9 0.0 reduce-scatter.2.cloned.1.call-start
  13.9 79.7 %all-reduce.5.cloned.1.call-done = (f32[1536,256]{0,1:T(8,128)}, f32[1536,256]{1,0:T(8,128)}) async-done(((f32[1536,256]{0,1:T(8,128)}, f32[1536,256]{1,0:T(8,128)}), (f32[1536,256]{0,1:T(8,128)}, f32[1536,256]{1,0:T(8,128)})) %all-reduce.5.cloned.1.call-update) | async-done | bytes 3145744 | tf_op jit(solution)/shard_map/psum | solution.py:71
  93.7 2.1 fusion.2
  95.8 0.0 copy-done.3
  95.8 0.0 copy-start.1
  95.8 0.6 convolution_add_fusion
  96.4 0.8 copy-done.1
  97.2 0.5 copy-done.2
  97.7 0.6 fusion.5
  98.3 0.6 convolution_add_fusion.1
  98.9 0.0 copy-start.5
  98.9 0.0 copy-start.6
  98.9 0.0 copy-start.7
  98.9 0.0 copy-start.8
  98.9 1.1 pad_maximum_fusion
  100.0 0.0 reduce-scatter.2.cloned.1.call-update
  100.0 0.0 all-gather.3.cloned.1.call-start
  100.1 28.0 %reduce-scatter.2.cloned.1.call-done = f32[64,1024]{1,0:T(8,128)} async-done(((f32[256,1024]{1,0:T(8,128)}), f32[64,1024]{1,0:T(8,128)}) %reduce-scatter.2.cloned.1.call-update) | async-done | bytes 262160 | tf_op jit(solution)/shard_map/reduce_scatter | solution.py:74
  128.0 0.0 copy-done.5
  128.0 1.9 add_divide_fusion
  129.9 10.1 %all_gather.13 = f32[256,512]{1,0:T(8,128)S(1)} all-gather(f32[64,512]{1,0:T(8,128)S(1)} %get-tuple-element.22), channel_id=1, replica_groups=mesh['fs'=4,'tp'=8] {'fs'}, dimensions={0}, use_global_device_ids=true | all-gather | bytes 655360 | tf_op jit(solution)/shard_map/all_gather | solution.py:81
  140.0 9.7 %all_gather.12 = f32[256,512]{1,0:T(8,128)S(1)} all-gather(f32[64,512]{1,0:T(8,128)S(1)} %get-tuple-element.28), channel_id=1, replica_groups=mesh['fs'=4,'tp'=8] {'fs'}, dimensions={0}, use_global_device_ids=true | all-gather | bytes 655360 | tf_op jit(solution)/shard_map/all_gather | solution.py:80
  149.7 2.3 multiply_reduce_fusion.1
  152.0 3.2 %multiply_reduce_fusion = (f32[]{:T(128)}, f32[512,512]{1,0:T(8,128)}) fusion(f32[256,512]{1,0:T(8,128)S(1)} %all_gather.13, bf16[2048,256]{1,0:T(8,128)(2,1)} %param.21, s32[]{:T(128)S(6)} %select_n.8), kind=kOutput, calls=%fused_computation.10 | convolution fusion | flops 805830656 | bytes 1835016 | tf_op jit(solution)/shard_map/dot_general | solution.py:84
  155.1 14.2 %all-reduce = (f32[]{:T(128)}, f32[]{:T(128)}) all-reduce(f32[]{:T(128)} %get-tuple-element.31, f32[]{:T(128)} %get-tuple-element.33), channel_id=1, replica_groups=mesh['fs'=4,'tp'=8] {'tp'}, use_global_device_ids=true, to_apply=%region_4.0 | all-reduce | flops 2 | bytes 16 | tf_op jit(solution)/shard_map/psum | solution.py:16
  169.4 9.5 %all-reduce.2 = (f32[]{:T(128)}, f32[]{:T(128)}) all-reduce(f32[]{:T(128)} %get-tuple-element.10, f32[]{:T(128)} %get-tuple-element.11), channel_id=1, replica_groups=mesh['fs'=4,'tp'=8] {'fs'}, use_global_device_ids=true, to_apply=%region_5.0 | all-reduce | flops 2 | bytes 16 | tf_op jit(solution)/shard_map/psum | solution.py:16
  179.6 3.1 %fusion.21 = (bf16[512,512]{1,0:T(8,128)(2,1)}, f32[512,512]{1,0:T(8,128)}, f32[512,512]{1,0:T(8,128)}) fusion(f32[512,512]{1,0:T(8,128)} %param.22, f32[512,512]{1,0:T(8,128)S(1)} %get-tuple-element.32, f32[]{:T(128)S(6)} %rsqrt.6), kind=kLoop, calls=%fused_computation.41 | loop fusion | flops 1048576 | bytes 4718596 | tf_op jit(solution)/shard_map/convert_element_type | solution.py:94
  182.7 0.0 all-gather.3.cloned.1.call-update
  182.7 0.0 all-gather.5.cloned.1.call-start
  182.7 1.6 copy.24
  185.0 3.1 %fusion.20 = (bf16[512,512]{1,0:T(8,128)(2,1)}, f32[512,512]{1,0:T(8,128)}, f32[512,512]{1,0:T(8,128)}) fusion(f32[512,512]{1,0:T(8,128)} %param.23, f32[512,512]{0,1:T(8,128)S(1)} %copy.24, f32[]{:T(128)S(6)} %rsqrt.7), kind=kLoop, calls=%fused_computation.40 | loop fusion | flops 1048576 | bytes 4718596 | tf_op jit(solution)/shard_map/convert_element_type | solution.py:95
  188.2 0.0 all-gather.5.cloned.1.call-update
  188.2 26.5 %all-gather.3.cloned.1.call-done = bf16[2048,512]{1,0:T(8,128)(2,1)} async-done(((bf16[512,512]{1,0:T(8,128)(2,1)}), bf16[2048,512]{1,0:T(8,128)(2,1)}) %all-gather.3.cloned.1.call-update) | async-done | bytes 2097168 | tf_op jit(solution)/shard_map/all_gather | solution.py:94
  214.7 37.3 %all-gather.5.cloned.1.call-done = bf16[512,2048]{1,0:T(8,128)(2,1)} async-done(((bf16[512,512]{1,0:T(8,128)(2,1)}), bf16[512,2048]{1,0:T(8,128)(2,1)}) %all-gather.5.cloned.1.call-update) | async-done | bytes 2097168 | tf_op jit(solution)/shard_map/all_gather | solution.py:95
  252.0 3.2 %copy.29 = bf16[2048,512]{1,0:T(8,128)(2,1)} copy(bf16[2048,512]{1,0:T(8,128)(2,1)} %all-gather.3.cloned.1.call-done) | data formatting | bytes 4194304
  255.2 1.3 copy.30
  (8 shorter events, 0.0 us)
Async XLA Ops:
  7.2 86.5 %copy-start = (bf16[1536,512]{1,0:T(8,128)(2,1)S(1)}, bf16[1536,512]{1,0:T(8,128)(2,1)}, u32[]{:S(2)}) copy-start(bf16[1536,512]{1,0:T(8,128)(2,1)} %param.19) | copy-start | bytes 4718596
  7.2 3.7 %copy-start.9 = (f32[256]{0:T(256)S(1)}, f32[256]{0:T(256)}, u32[]{:S(2)}) copy-start(f32[256]{0:T(256)} %param.17) | copy-start | bytes 3076
  7.2 3.7 %copy-start.11 = (bf16[1536,256]{1,0:T(8,128)(2,1)S(1)}, bf16[1536,256]{1,0:T(8,128)(2,1)}, u32[]{:S(2)}) copy-start(bf16[1536,256]{1,0:T(8,128)(2,1)} %param.16) | copy-start | bytes 2359300
  7.2 3.7 %copy-start.10 = (bf16[1536,256]{1,0:T(8,128)(2,1)S(1)}, bf16[1536,256]{1,0:T(8,128)(2,1)}, u32[]{:S(2)}) copy-start(bf16[1536,256]{1,0:T(8,128)(2,1)} %param.15) | copy-start | bytes 2359300
  7.2 86.4 %all-reduce.5.cloned.1.call-start = ((), (), s32[]{:S(2)}) async-start(), calls=%async_computation.4 | async-start | bytes 6291456 | tf_op jit(solution)/shard_map/psum | solution.py:71
  13.9 114.1 %reduce-scatter.2.cloned.1.call-start = ((), (), s32[]{:S(2)}) async-start(), calls=%async_computation.1 | async-start | bytes 1310720 | tf_op jit(solution)/shard_map/reduce_scatter | solution.py:74
  93.7 2.1 copy-start.3
  95.8 1.4 copy-start.1
  95.8 1.9 copy-start.2
  98.9 29.2 %copy-start.5 = (f32[64,512]{1,0:T(8,128)S(1)}, f32[64,512]{1,0:T(8,128)}, u32[]{:S(2)}) copy-start(f32[64,512]{1,0:T(8,128)} %param.27) | copy-start | bytes 393220
  98.9 29.2 %copy-start.6 = (f32[64,512]{1,0:T(8,128)S(1)}, f32[64,512]{1,0:T(8,128)}, u32[]{:S(2)}) copy-start(f32[64,512]{1,0:T(8,128)} %param.26) | copy-start | bytes 393220
  98.9 29.1 %copy-start.7 = (f32[64,512]{1,0:T(8,128)S(1)}, f32[64,512]{1,0:T(8,128)}, u32[]{:S(2)}) copy-start(f32[64,512]{1,0:T(8,128)} %param.25) | copy-start | bytes 393220
  98.9 29.1 %copy-start.8 = (f32[64,512]{1,0:T(8,128)S(1)}, f32[64,512]{1,0:T(8,128)}, u32[]{:S(2)}) copy-start(f32[64,512]{1,0:T(8,128)} %param.24) | copy-start | bytes 393220
  100.0 114.7 %all-gather.3.cloned.1.call-start = ((), (), s32[]{:S(2)}) async-start(), calls=%async_computation.2 | async-start | bytes 2621440 | tf_op jit(solution)/shard_map/all_gather | solution.py:94
  182.7 69.3 %all-gather.5.cloned.1.call-start = ((), (), s32[]{:S(2)}) async-start(), calls=%async_computation.3 | async-start | bytes 2621440 | tf_op jit(solution)/shard_map/all_gather | solution.py:95
  252.0 3.2 %copy-start.4 = (bf16[512,2048]{1,0:T(8,128)(2,1)S(1)}, bf16[512,2048]{1,0:T(8,128)(2,1)}, u32[]{:S(2)}) copy-start(bf16[512,2048]{1,0:T(8,128)(2,1)} %all-gather.5.cloned.1.call-done) | copy-start | bytes 6291460
Sparse Core Ops, SparseCore 0:
  14.0 79.5 all-reduce.4
  100.1 27.8 reduce-scatter.1
  182.8 31.8 all-gather.2
  216.9 35.0 all-gather.4
